TPU v7x, 32 devices: a whole 2x2x4 slice. The times are simulated.
32 devices in a mesh: sp: 16 (over z, y, x), tp: 2 (over core).
Axes of the slice: x: 2, y: 2, z: 4, core: 2. Of those that a mesh axis runs over, the one named last changes fastest.
Arguments:
- queries: bfloat16 [4096, 1024], P('sp', 'tp'), may hold values from -6 to 6
- key_vectors: bfloat16 [4096, 1024], P('sp', 'tp'), may hold values from -6 to 6
- value_vectors: bfloat16 [4096, 1024], P('sp', 'tp'), may hold values from -6 to 6
- gate_inputs: bfloat16 [4096, 1024], P('sp', 'tp'), may hold values from -6 to 6
- log_decay: float32 [4096, 16], P('sp', 'tp'), may hold values from -1 to 0
- head_gain: float32 [1024], P('tp'), may hold values from 0.1 to 1.9
- out_weight: bfloat16 [1024, 2048], P('tp'), may hold values from -0.1875 to 0.1875
- residual: bfloat16 [4096, 2048], P(('sp', 'tp')), may hold values from -6 to 6
- norm_gain: float32 [2048], replicated, may hold values from 0.1 to 1.9
- expert_ids: int32 [4096, 2], P(('sp', 'tp')), may hold values from 0 to 15, all different within a row; in each aligned block of 128 rows (0 to 127, 128 to 255, ...) at most 32 rows name the same one
- expert_weights: float32 [4096, 2], P(('sp', 'tp')), may hold values from 0.2 to 1
- gate_experts: bfloat16 [16, 2048, 3584], P('sp', None, 'tp'), may hold values from -0.125 to 0.125
- up_experts: bfloat16 [16, 2048, 3584], P('sp', None, 'tp'), may hold values from -0.125 to 0.125
- down_experts: bfloat16 [16, 3584, 2048], P('sp', 'tp'), may hold values from -0.09375 to 0.09375
Outputs:
- layer_out: bfloat16 [4096, 2048], P(('sp', 'tp'))
Inputs may be any that keep to these rules, and one draw needn't show every extreme that they name: `expert_ids`: the 2 experts of a token differ. No expert is named more than 32 times in the rows of one device, and in some device some expert is named exactly 32 times.
All inputs are finite; a program needn't handle non-finite values.
Results may differ from a plain program's by a relative error of at most 0.014.
Values may be sent and summed in bfloat16 or wider, within the bound.
No kernel may reach another device: no remote copies, remote signals or barrier semaphores. Data moves between devices by JAX's collectives and lax.ppermute only.
A program may use at most 128 MiB of HBM per device.

v0:
```python
import functools

import jax
import jax.numpy as jnp
import numpy as np
from jax import lax
from jax.experimental import pallas as pl
from jax.experimental.pallas import tpu as pltpu
from jax.sharding import PartitionSpec as P


BF16 = jnp.bfloat16
F32 = jnp.float32
LANES = 128
NEG = -1e30


def dot(a, b, dims=((1,), (0,)), precision=None):
    return lax.dot_general(a, b, (dims, ((), ())), precision=precision, preferred_element_type=F32)


def params(vmem):
    return pltpu.CompilerParams(vmem_limit_bytes=vmem * 1024 * 1024)


def call(kernel, outs, args, vmem, **static):
    return pl.pallas_call(
        functools.partial(kernel, **static) if static else kernel,
        out_shape=[jax.ShapeDtypeStruct(s, d) for s, d in outs],
        compiler_params=params(vmem),
    )(*args)


def staged_call(kernel, outs, args, vmem, **static):
    count, outputs = len(args), len(outs)

    def body(*refs):
        given, results = refs[:count], refs[count : count + outputs]
        local, sems = refs[count + outputs : -1], refs[-1]
        copies = [
            pltpu.make_async_copy(src, dst, sems.at[i])
            for i, (src, dst) in enumerate(zip(given, local))
        ]
        for copy in copies:
            copy.start()
        for copy in copies:
            copy.wait()
        kernel(*local, *results, **static)

    return pl.pallas_call(
        body,
        in_specs=[pl.BlockSpec(memory_space=pltpu.HBM)] * count,
        out_shape=[jax.ShapeDtypeStruct(s, d) for s, d in outs],
        scratch_shapes=[pltpu.VMEM(a.shape, a.dtype) for a in args]
        + [pltpu.SemaphoreType.DMA((count,))],
        compiler_params=params(vmem),
    )(*[pltpu.with_memory_space_constraint(a, pltpu.HBM) for a in args])


def lane_iota(rows, lanes=LANES):
    return lax.broadcasted_iota(jnp.int32, (rows, lanes), 1)


def row_iota(rows, lanes=LANES):
    return lax.broadcasted_iota(jnp.int32, (rows, lanes), 0)


def angles(base_ref, cos_ref, sin_ref):
    place = lax.axis_index("sp")
    base = base_ref[place]
    cos_base, sin_base = base[0:1, :], base[1:2, :]
    cos_t, sin_t = cos_ref[...], sin_ref[...]
    return cos_base * cos_t - sin_base * sin_t, sin_base * cos_t + cos_base * sin_t


def turn(x, cos, sin, size):
    half = size // 2
    first = lane_iota(x.shape[0]) % size < half
    other = jnp.where(first, pltpu.roll(x, LANES - half, 1), pltpu.roll(x, half, 1))
    return x * cos + other * sin


def cumulative_of(decay):
    rows = decay.shape[1]
    lower = (row_iota(rows, rows) >= lane_iota(rows, rows)).astype(F32)
    return dot(lower, decay, ((1,), (1,)), precision=lax.Precision.HIGHEST)


def spread(table, pair, rows, size):
    each = LANES // size
    lane = lane_iota(rows)
    wide = jnp.broadcast_to(table[:, pair * each : pair * each + 1], (rows, LANES))
    for i in range(1, each):
        wide = jnp.where(lane >= i * size, table[:, pair * each + i : pair * each + i + 1], wide)
    return wide


def state_kernel(k_ref, v_ref, decay_ref, base_ref, cos_ref, sin_ref, out_ref, *, size):
    rows, channels = k_ref.shape
    pairs = channels // LANES
    each = LANES // size
    cos, sin = angles(base_ref, cos_ref, sin_ref)
    cumulative = cumulative_of(decay_ref[...])
    total = cumulative[rows - 1 : rows, :]
    end = jnp.exp(total - cumulative)
    lane = lane_iota(size)
    for pair in range(pairs):
        cols = slice(pair * LANES, (pair + 1) * LANES)
        key = turn(k_ref[:, cols].astype(F32), cos, sin, size) * size ** (-0.5)
        key = (key * spread(end, pair, rows, size)).astype(BF16)
        full = dot(key, v_ref[:, cols], ((0,), (0,)))
        packed = full[0:size]
        for i in range(1, each):
            packed = jnp.where(lane >= i * size, full[i * size : (i + 1) * size], packed)
        out_ref[pair * size : (pair + 1) * size, :] = packed.astype(BF16)
    store_totals(out_ref, [spread(total, pair, 1, size) for pair in range(pairs)], size)


def store_totals(out_ref, totals, size):
    pairs = len(totals)
    low = [h - h.astype(BF16).astype(F32) for h in totals]
    fill = [jnp.zeros((16 - 2 * pairs, LANES), F32)]
    out_ref[pairs * size : pairs * size + 16, :] = jnp.concatenate(totals + low + fill, 0).astype(
        BF16
    )


def within_kernel(
    q_ref,
    k_ref,
    v_ref,
    decay_ref,
    base_ref,
    cos_ref,
    sin_ref,
    gain_ref,
    gate_ref,
    within_ref,
    scaled_ref,
    factor_ref,
    *,
    size,
):
    rows, channels = k_ref.shape
    pairs = channels // LANES
    each = LANES // size
    cos, sin = angles(base_ref, cos_ref, sin_ref)
    decay = decay_ref[...]
    cumulative = cumulative_of(decay)
    upper = (row_iota(rows, rows) <= lane_iota(rows, rows)).astype(F32)
    across = dot(decay, upper, precision=lax.Precision.HIGHEST)
    grown = jnp.exp(cumulative)
    causal = row_iota(rows, rows) >= lane_iota(rows, rows)
    lane = lane_iota(rows)
    for pair in range(pairs):
        cols = slice(pair * LANES, (pair + 1) * LANES)
        gate = gate_ref[:, cols].astype(F32)
        factor_ref[:, cols] = gain_ref[:, cols] * (gate / (1.0 + jnp.exp(-gate)))
        key = turn(k_ref[:, cols].astype(F32), cos, sin, size) * size ** (-0.5)
        query = turn(q_ref[:, cols].astype(F32), cos, sin, size)
        scaled_ref[:, cols] = (query * spread(grown, pair, rows, size)).astype(BF16)
        query = query.astype(BF16)
        value = v_ref[:, cols]
        result = jnp.zeros((rows, LANES), F32)
        for i in range(each):
            head = pair * each + i
            mine = (lane >= i * size) & (lane < (i + 1) * size)
            scores = dot(query, jnp.where(mine, key, 0.0).astype(BF16), ((1,), (1,)))
            gap = cumulative[:, head : head + 1] - across[head : head + 1, :]
            weight = jnp.exp(jnp.where(causal, gap, NEG))
            got = dot((scores * weight).astype(BF16), value)
            result = jnp.where(mine, got, result)
        within_ref[:, cols] = result


def level_shifts(count, stride, radix, last):
    out = []
    for k in range(1, radix):
        out.append([])
        for j in range(count):
            d = (j // stride) % radix
            if not (last and d + k >= radix):
                out[-1].append((j, j + ((d + k) % radix - d) * stride))
    return out


def radices_of(count):
    out = []
    while count > 1:
        radix = next(r for r in (4, 2, 3, count) if count % r == 0)
        out.append(radix)
        count //= radix
    return out


def state_of(ref, pair, size):
    return ref[pair * size : (pair + 1) * size, :].astype(F32)


def total_of(tail, pair, pairs):
    return tail[pair : pair + 1, :] + tail[pairs + pair : pairs + pair + 1, :]


def earlier(got_refs, tails, pair, pairs, size, digit, below=False):
    state = jnp.zeros((size, LANES), F32)
    total = jnp.zeros((1, LANES), F32)
    for k, (ref, tail) in enumerate(zip(got_refs, tails), 1):
        use = jnp.where(digit < k if below else digit >= k, 1.0, 0.0)
        state = state + use * jnp.exp(total) * state_of(ref, pair, size)
        total = total + use * total_of(tail, pair, pairs)
    return state, total


def level_kernel(own_ref, before_ref, *refs, pairs, size, stride, radix):
    got_refs, (all_ref, sofar_ref) = refs[: radix - 1], refs[radix - 1 :]
    digit = (lax.axis_index("sp") // stride) % radix
    base = pairs * size
    tails = [ref[base : base + 16, :].astype(F32) for ref in got_refs]
    own_tail = own_ref[base : base + 16, :].astype(F32)
    totals = []
    for pair in range(pairs):
        state, total = earlier(got_refs, tails, pair, pairs, size, digit)
        rest, behind = earlier(got_refs, tails, pair, pairs, size, digit, below=True)
        rest = rest + jnp.exp(behind) * state_of(own_ref, pair, size)
        behind = behind + total_of(own_tail, pair, pairs)
        rest = rest + jnp.exp(behind) * state
        rows = slice(pair * size, (pair + 1) * size)
        all_ref[rows, :] = rest.astype(BF16)
        totals.append(behind + total)
        old = before_ref[base + pair : base + pair + 1, :]
        sofar_ref[rows, :] = before_ref[rows, :] + jnp.exp(old) * state
        sofar_ref[base + pair : base + pair + 1, :] = old + total
    sofar_ref[base + pairs : base + 16, :] = jnp.zeros((16 - pairs, LANES), F32)
    store_totals(all_ref, totals, size)


def normed_kernel(
    within_ref, scaled_ref, factor_ref, before_ref, *refs, size, stride, radix, core_axis
):
    got_refs, (mine_ref, theirs_ref, rows_ref) = refs[: radix - 1], refs[radix - 1 :]
    rows, channels = within_ref.shape
    pairs = channels // LANES
    each = LANES // size
    base = pairs * size
    digit = (lax.axis_index("sp") // stride) % radix
    tails = [ref[base : base + 16, :].astype(F32) for ref in got_refs]
    lane = lane_iota(rows)
    lane_s = lane_iota(size)
    for pair in range(pairs):
        cols = slice(pair * LANES, (pair + 1) * LANES)
        state, _ = earlier(got_refs, tails, pair, pairs, size, digit)
        old = before_ref[base + pair : base + pair + 1, :]
        packed = before_ref[pair * size : (pair + 1) * size, :] + jnp.exp(old) * state
        blocks = [
            jnp.where((lane_s >= i * size) & (lane_s < (i + 1) * size), packed, 0.0)
            for i in range(each)
        ]
        incoming = jnp.concatenate(blocks, 0).astype(BF16)
        retained = within_ref[:, cols] + dot(scaled_ref[:, cols], incoming)
        squares = retained * retained
        mean = jnp.zeros((rows, LANES), F32)
        for i in range(each):
            mine = (lane >= i * size) & (lane < (i + 1) * size)
            part = jnp.sum(jnp.where(mine, squares, 0.0), axis=1, keepdims=True) * (1.0 / size)
            mean = jnp.where(mine, part, mean)
        out = retained * lax.rsqrt(mean + 1e-06) * factor_ref[:, cols]
        rows_ref[:, cols] = out.astype(BF16)
    tokens = mine_ref.shape[0]
    core = lax.axis_index(core_axis)
    mine_ref[...] = rows_ref[pl.ds(pl.multiple_of(core * tokens, tokens), tokens), :]
    theirs_ref[...] = rows_ref[pl.ds(pl.multiple_of((1 - core) * tokens, tokens), tokens), :]


def meta_of(meta_ref, top):
    meta = meta_ref[...].T
    first = meta[:, 2 * top : 2 * top + 1]
    return meta[:, :top] - first, meta[:, top : 2 * top]


def slots_of(ids, capacity, slots):
    tokens = ids.shape[0]
    lane = lane_iota(tokens).astype(F32)
    named = [lane == ids[:, j : j + 1] for j in range(ids.shape[1])]
    member = functools.reduce(jnp.logical_or, named).astype(BF16)
    strict = (row_iota(tokens, tokens) > lane_iota(tokens, tokens)).astype(BF16)
    rank = dot(strict, member)
    place = lane_iota(tokens, slots).astype(F32)
    out = []
    for j, hit in enumerate(named):
        slot = ids[:, j : j + 1] * capacity + jnp.sum(jnp.where(hit, rank, 0.0), 1, keepdims=True)
        out.append(place == slot)
    return out


def dispatch_kernel(
    a_ref, b_ref, wa_ref, wb_ref, res_ref, gain_ref, meta_ref, mixed_ref, out_ref, *, capacity, top
):
    projected = dot(a_ref[...], wa_ref[...]).astype(BF16).astype(F32)
    projected = projected + dot(b_ref[...], wb_ref[...]).astype(BF16).astype(F32)
    mixed = (res_ref[...].astype(F32) + projected).astype(BF16)
    mixed_ref[...] = mixed
    wide = mixed.astype(F32)
    scale = lax.rsqrt(jnp.mean(wide * wide, axis=1, keepdims=True) + 1e-06)
    rows = (wide * scale * gain_ref[...]).astype(BF16)
    ids, _ = meta_of(meta_ref, top)
    hot = functools.reduce(jnp.logical_or, slots_of(ids, capacity, out_ref.shape[0]))
    out_ref[...] = dot(hot.astype(BF16), rows, ((0,), (0,))).astype(BF16)


def expert_kernel(
    own_ref, oth_ref, gate_ref, up_ref, down_ref, pown_ref, poth_ref, hidden_ref, *, first
):
    step = pl.program_id(0)
    count = own_ref.shape[0]
    tile = gate_ref.shape[1]

    @pl.when(step < first)
    def _():
        rows = jnp.concatenate([own_ref[...], oth_ref[...]], 0)
        gate = dot(rows, gate_ref[...])
        up = dot(rows, up_ref[...])
        hidden = (gate / (1.0 + jnp.exp(-gate)) * up).astype(BF16)
        hidden_ref[:, pl.ds(pl.multiple_of(step * tile, tile), tile)] = hidden

    @pl.when(step >= first)
    def _():
        part = dot(hidden_ref[...], down_ref[...])
        pown_ref[...] = part[:count].astype(BF16)
        poth_ref[...] = part[count:].astype(BF16)


def experts_call(own, oth, gate, up, down):
    rows, width = own.shape
    hidden = gate.shape[2]
    tile = next(t for t in (256, 128, hidden) if hidden % t == 0)
    wide = next(t for t in (512, 256, 128, width) if width % t == 0)
    first, last = hidden // tile, width // wide
    whole = pl.BlockSpec((rows, width), lambda i: (0, 0))
    part = pl.BlockSpec((rows, wide), lambda i: (0, jnp.maximum(i - first, 0)))
    entry = pl.BlockSpec((None, width, tile), lambda i: (0, 0, jnp.minimum(i, first - 1)))
    return pl.pallas_call(
        functools.partial(expert_kernel, first=first),
        grid=(first + last,),
        in_specs=[
            whole,
            whole,
            entry,
            entry,
            pl.BlockSpec((None, hidden, wide), lambda i: (0, 0, jnp.maximum(i - first, 0))),
        ],
        out_specs=[part, part],
        out_shape=[jax.ShapeDtypeStruct((rows, width), BF16)] * 2,
        scratch_shapes=[pltpu.VMEM((2 * rows, hidden), BF16)],
        compiler_params=params(32),
        cost_estimate=pl.CostEstimate(
            flops=2 * rows * 6 * width * hidden,
            bytes_accessed=6 * width * hidden,
            transcendentals=2 * rows * hidden,
        ),
    )(own, oth, *[pltpu.with_memory_space_constraint(w, pltpu.HBM) for w in (gate, up, down)])


def gather_sum(ret, ids, weights, capacity):
    hots = slots_of(ids, capacity, ret.shape[0])
    total = None
    for j, hot in enumerate(hots):
        part = dot(hot.astype(BF16), ret) * weights[:, j : j + 1]
        total = part if total is None else total + part
    return total


def back_kernel(ret_ref, meta_ref, out_ref, *, capacity, top):
    ids, weights = meta_of(meta_ref, top)
    out_ref[...] = gather_sum(ret_ref[...], ids, weights, capacity).astype(out_ref.dtype)


def final_kernel(mixed_ref, part_ref, far_ref, out_ref):
    total = part_ref[...] + far_ref[...].astype(F32)
    out_ref[...] = (mixed_ref[...].astype(F32) + total).astype(BF16)


def shards(
    queries,
    key_vectors,
    value_vectors,
    gate_inputs,
    log_decay,
    head_gain,
    out_weight,
    residual,
    norm_gain,
    expert_ids,
    expert_weights,
    gate_experts,
    up_experts,
    down_experts,
):
    tok_dev, channels = queries.shape
    heads = log_decay.shape[1]
    size = channels // heads
    pairs = channels // LANES
    tokens, width = residual.shape
    count = lax.axis_size("sp")
    cores = lax.axis_size("tp")
    half = count // 2
    capacity = 2 * tok_dev // count
    place = lax.axis_index("sp")
    across = [(j, (j + half) % count) for j in range(count)]
    swap = [(c, cores - 1 - c) for c in range(cores)]
    groups = [list(range(half)), list(range(half, count))]

    top = expert_ids.shape[1]

    def meta_for(where):
        first = jnp.broadcast_to((where // half * half).astype(F32), (1, tokens))
        fill = jnp.zeros((8 - 2 * top - 1, tokens), F32)
        return jnp.concatenate([expert_ids.T.astype(F32), expert_weights.T, first, fill], 0)

    far_res = lax.ppermute(residual, "sp", across)
    other_weight = lax.ppermute(out_weight, "tp", swap)
    meta = meta_for(place)
    far_meta = lax.ppermute(meta_for((place + half) % count), "sp", across)

    lane = np.arange(LANES) % size
    freq = 10000.0 ** (-(lane % (size // 2)) / (size // 2))
    sign = np.where(lane < size // 2, -1.0, 1.0)
    turns = np.arange(tok_dev)[:, None] * freq
    starts = (np.arange(count) * tok_dev)[:, None] * freq
    cos_t, sin_t = jnp.asarray(np.cos(turns), F32), jnp.asarray(np.sin(turns) * sign, F32)
    bases = np.zeros((count, 8, LANES), np.float32)
    bases[:, 0], bases[:, 1] = np.cos(starts), np.sin(starts) * sign
    bases = jnp.asarray(bases)
    decay = log_decay.T
    (own,) = staged_call(
        state_kernel,
        [((pairs * size + 16, LANES), BF16)],
        (key_vectors, value_vectors, decay, bases, cos_t, sin_t),
        12,
        size=size,
    )
    within, scaled, factor = staged_call(
        within_kernel,
        [((tok_dev, channels), F32), ((tok_dev, channels), BF16), ((tok_dev, channels), F32)],
        (
            queries,
            key_vectors,
            value_vectors,
            decay,
            bases,
            cos_t,
            sin_t,
            head_gain[None, :],
            gate_inputs,
        ),
        20,
        size=size,
    )
    levels = radices_of(count)
    before = jnp.zeros((pairs * size + 16, LANES), F32)
    stride = 1
    for level, radix in enumerate(levels):
        last = level == len(levels) - 1
        got = [lax.ppermute(own, "sp", p) for p in level_shifts(count, stride, radix, last)]
        if not last:
            own, before = call(
                level_kernel,
                [(own.shape, BF16), (before.shape, F32)],
                (own, before, *got),
                8,
                pairs=pairs,
                size=size,
                stride=stride,
                radix=radix,
            )
            stride *= radix
    mine, theirs = pl.pallas_call(
        functools.partial(normed_kernel, size=size, stride=stride, radix=radix, core_axis="tp"),
        out_shape=[jax.ShapeDtypeStruct((tokens, channels), BF16)] * 2,
        scratch_shapes=[pltpu.VMEM((tok_dev, channels), BF16)],
        compiler_params=params(12),
        name="normed",
    )(within, scaled, factor, before, *got)

    axes = ("sp", "tp")
    index = [(j, c) for j in range(count) for c in range(cores)]
    flip = [(j * cores + c, j * cores + cores - 1 - c) for j, c in index]
    same = [(j * cores + c, (j + half) % count * cores + c) for j, c in index]
    cross = [(j * cores + c, (j + half) % count * cores + cores - 1 - c) for j, c in index]
    near = lax.ppermute(theirs, axes, flip)
    far_a = lax.ppermute(mine, axes, same)
    far_b = lax.ppermute(theirs, axes, cross)

    def dispatch(a, b, res, who):
        mixed, out = call(
            dispatch_kernel,
            [((tokens, width), BF16), ((half * capacity, width), BF16)],
            (a, b, out_weight, other_weight, res, norm_gain[None, :], who),
            20,
            capacity=capacity,
            top=top,
        )
        return mixed, out.reshape(half, capacity, width)

    def exchange(x):
        return lax.all_to_all(
            x, "sp", split_axis=0, concat_axis=0, tiled=True, axis_index_groups=groups
        )

    def run(received):
        rows = received.reshape(half * capacity, width)
        oth = lax.ppermute(rows, "tp", swap)
        p_own, p_oth = experts_call(rows, oth, gate_experts, up_experts, down_experts)
        back = lax.ppermute(p_oth, "tp", swap)
        total = (p_own.astype(F32) + back.astype(F32)).astype(BF16)
        return total.reshape(half, capacity, width)

    def back(returned, who, dtype):
        (out,) = call(
            back_kernel,
            [((tokens, width), dtype)],
            (returned.reshape(half * capacity, width), who),
            16,
            capacity=capacity,
            top=top,
        )
        return out

    mixed, out_near = dispatch(mine, near, residual, meta)
    got_near = exchange(out_near)
    _, out_far = dispatch(far_a, far_b, far_res, far_meta)
    got_far = exchange(out_far)
    ret_near = exchange(run(got_near))
    ret_far = exchange(run(got_far))
    part = back(ret_near, meta, F32)
    far_sum = back(ret_far, far_meta, BF16)
    arrived = lax.ppermute(far_sum, "sp", across)
    (out,) = call(final_kernel, [((tokens, width), BF16)], (mixed, part, arrived), 12)
    return out


def solution(mesh):
    return jax.shard_map(
        shards,
        mesh=mesh,
        in_specs=(
            P("sp", "tp"),
            P("sp", "tp"),
            P("sp", "tp"),
            P("sp", "tp"),
            P("sp", "tp"),
            P("tp"),
            P("tp", None),
            P(("sp", "tp"), None),
            P(),
            P(("sp", "tp"), None),
            P(("sp", "tp"), None),
            P("sp", None, "tp"),
            P("sp", None, "tp"),
            P("sp", "tp", None),
        ),
        out_specs=P(("sp", "tp"), None),
        check_vma=False,
    )
```

profile of v0, /device:TPU:0, one launch (start us, length us, event | category | flops | bytes accessed | tf_op | source)
XLA Modules:
  0.0 172.7 jit_solution(2621917660792830836)
XLA Ops:
  0.5 2.3 %shard_map.164.own_ref = bf16[272,128]{1,0:T(8,128)(2,1)S(1)} custom-call(bf16[256,512]{1,0:T(8,128)(2,1)} %refs_0_.3, bf16[256,512]{1,0:T(8,128)(2,1)} %refs_1_.3, f32[8,256]{1,0:T(8,128)} %bitcast.27, f32[16,8,128]{2,1,0:T(8,128)} %constant.53.clone.refs_4_.refs_3_, f32[256,128]{1,0:T(8,128)} %constant.51.clone.refs_5_.refs_4_, ...), custom_call_target="tpu_custom_call" | custom-call | tf_op jit(solution)/shard_map/pallas_call | solution.py:50
  2.8 3.5 %collective-permute-start.2 = (bf16[272,128]{1,0:T(8,128)(2,1)S(1)}, bf16[272,128]{1,0:T(8,128)(2,1)S(1)}, u32[]{:S(2)}, u32[]{:S(2)}) collective-permute-start(bf16[272,128]{1,0:T(8,128)(2,1)S(1)} %shard_map.164.own_ref), channel_id=1, source_target_pairs={{0,6},{2,0},{4,2},{6,4},{8,14},{10,8},{12,10},{14,12},{16,22},{18,... | collective-permute-start | bytes 208904 | tf_op jit(solution)/shard_map/ppermute | solution.py:463
  7.4 2.6 %collective-permute-start.12 = (bf16[128,2048]{1,0:T(8,128)(2,1)}, bf16[128,2048]{1,0:T(8,128)(2,1)S(1)}, u32[]{:S(2)}, u32[]{:S(2)}) collective-permute-start(bf16[128,2048]{1,0:T(8,128)(2,1)} %res_ref.1), channel_id=1, source_target_pairs={{0,16},{2,18},{4,20},{6,22},{8,24},{10,26},{12,28},{14,30},{16,0},... | collective-permute-start | bytes 1572872 | tf_op jit(solution)/shard_map/ppermute | solution.py:419
  10.0 2.1 %collective-permute-done.1.refs_1_ = bf16[272,128]{1,0:T(8,128)(2,1)S(1)} collective-permute-done((bf16[272,128]{1,0:T(8,128)(2,1)S(1)}, bf16[272,128]{1,0:T(8,128)(2,1)S(1)}, u32[]{:S(2)}, u32[]{:S(2)}) %collective-permute-start.1) | collective-permute-done | bytes 69664 | tf_op jit(solution)/shard_map/ppermute | solution.py:463
  12.3 5.5 %collective-permute-start.5 = (bf16[272,128]{1,0:T(8,128)(2,1)S(1)}, bf16[272,128]{1,0:T(8,128)(2,1)S(1)}, u32[]{:S(2)}, u32[]{:S(2)}) collective-permute-start(bf16[272,128]{1,0:T(8,128)(2,1)S(1)} %get-tuple-element.23), channel_id=1, source_target_pairs={{0,24},{2,26},{4,28},{6,30},{1,25},{3,27},{5,29},{7,31}} | collective-permute-start | bytes 208904 | tf_op jit(solution)/shard_map/ppermute | solution.py:463
  19.1 2.5 %collective-permute-start.3 = (bf16[272,128]{1,0:T(8,128)(2,1)S(1)}, bf16[272,128]{1,0:T(8,128)(2,1)S(1)}, u32[]{:S(2)}, u32[]{:S(2)}) collective-permute-start(bf16[272,128]{1,0:T(8,128)(2,1)S(1)} %get-tuple-element.23), channel_id=1, source_target_pairs={{0,8},{2,10},{4,12},{6,14},{8,16},{10,18},{12,20},{14,22},{16,24},... | collective-permute-start | bytes 208904 | tf_op jit(solution)/shard_map/ppermute | solution.py:463
  22.5 3.1 %shard_map.163 = (f32[256,512]{1,0:T(8,128)S(1)}, bf16[256,512]{1,0:T(8,128)(2,1)S(1)}, f32[256,512]{1,0:T(8,128)S(1)}) custom-call(bf16[256,512]{1,0:T(8,128)(2,1)} %refs_0_.2, bf16[256,512]{1,0:T(8,128)(2,1)} %refs_0_.3, bf16[256,512]{1,0:T(8,128)(2,1)} %refs_1_.3, f32[8,256]{1,0:T(8,128)} %bitcast.28, f32[16,8,128]{2,1,0:T(8,128)} %constant.53.clone.refs_4_.refs_3_, ...), custom_call_target="tpu_custom_call" | custom-call | tf_op jit(solution)/shard_map/pallas_call | solution.py:50
  26.3 16.1 %collective-permute-start.10 = (bf16[128,512]{1,0:T(8,128)(2,1)S(1)}, bf16[128,512]{1,0:T(8,128)(2,1)S(1)}, u32[]{:S(2)}, u32[]{:S(2)}) collective-permute-start(bf16[128,512]{1,0:T(8,128)(2,1)S(1)} %get-tuple-element.24.a_ref), channel_id=1, source_target_pairs={{0,16},{1,17},{2,18},{3,19},{4,20},{5,21},{6,22},{7,23},{8,24},{9,... | collective-permute-start | bytes 393224 | tf_op jit(solution)/shard_map/ppermute | solution.py:490
  42.5 2.3 %collective-permute-start.13 = (f32[8,128]{1,0:T(8,128)S(1)}, f32[8,128]{1,0:T(8,128)S(1)}, u32[]{:S(2)}, u32[]{:S(2)}) collective-permute-start(f32[8,128]{1,0:T(8,128)S(1)} %get-tuple-element.33), channel_id=1, source_target_pairs={{0,16},{2,18},{4,20},{6,22},{8,24},{10,26},{12,28},{14,30},{16,0},... | collective-permute-start | bytes 12296 | tf_op jit(solution)/shard_map/ppermute | solution.py:422
  44.8 9.9 %collective-permute-done.13.meta_ref = f32[8,128]{1,0:T(8,128)S(1)} collective-permute-done((f32[8,128]{1,0:T(8,128)S(1)}, f32[8,128]{1,0:T(8,128)S(1)}, u32[]{:S(2)}, u32[]{:S(2)}) %collective-permute-start.13) | collective-permute-done | bytes 4128 | tf_op jit(solution)/shard_map/ppermute | solution.py:422
  54.7 3.2 %shard_map.169 = (bf16[128,2048]{1,0:T(8,128)(2,1)}, bf16[256,2048]{1,0:T(8,128)(2,1)S(1)}) custom-call(bf16[128,512]{1,0:T(8,128)(2,1)S(1)} %collective-permute-done.10.a_ref, bf16[128,512]{1,0:T(8,128)(2,1)S(1)} %collective-permute-done.11.b_ref, bf16[512,2048]{1,0:T(8,128)(2,1)S(1)} %copy-done, bf16[512,2048]{1,0:T(8,128)(2,1)} %collective-permute-done.7.wb_ref, ...), custom_call_target="tpu_custom_call" | custom-call | tf_op jit(solution)/shard_map/pallas_call | solution.py:27
  57.9 18.6 %all_to_all.20 = bf16[8,32,2048]{2,1,0:T(8,128)(2,1)S(1)} all-to-all(bf16[8,32,2048]{2,1,0:T(8,128)(2,1)S(1)} %bitcast.23), channel_id=1, replica_groups={{0,2,4,6,8,10,12,14},{16,18,20,22,24,26,28,30},{1,3,5,7,9,11,13,15},{17..., dimensions={0} | all-to-all | bytes 2097152 | tf_op jit(solution)/shard_map/all_to_all | solution.py:505
  77.0 2.3 %collective-permute-done.6.b_ref = bf16[128,512]{1,0:T(8,128)(2,1)S(1)} collective-permute-done((bf16[128,512]{1,0:T(8,128)(2,1)S(1)}, bf16[128,512]{1,0:T(8,128)(2,1)S(1)}, u32[]{:S(2)}, u32[]{:S(2)}) %collective-permute-start.6) | collective-permute-done | bytes 131104 | tf_op jit(solution)/shard_map/ppermute | solution.py:489
  79.4 3.1 %shard_map.166 = (bf16[128,2048]{1,0:T(8,128)(2,1)S(1)}, bf16[256,2048]{1,0:T(8,128)(2,1)S(1)}) custom-call(bf16[128,512]{1,0:T(8,128)(2,1)S(1)} %get-tuple-element.24.a_ref, bf16[128,512]{1,0:T(8,128)(2,1)S(1)} %collective-permute-done.6.b_ref, bf16[512,2048]{1,0:T(8,128)(2,1)S(1)} %copy-done, bf16[512,2048]{1,0:T(8,128)(2,1)} %collective-permute-done.7.wb_ref, ...), custom_call_target="tpu_custom_call" | custom-call | tf_op jit(solution)/shard_map/pallas_call | solution.py:27
  84.2 3.6 %all-to-all-start = ((bf16[8,32,2048]{2,1,0:T(8,128)(2,1)}), bf16[8,32,2048]{2,1,0:T(8,128)(2,1)S(1)}, u32[]{:S(2)}, u32[]{:S(2)}) async-start(bf16[8,32,2048]{2,1,0:T(8,128)(2,1)} %bitcast.22), calls=%async_computation | async-start | bytes 2097152 | tf_op jit(solution)/shard_map/all_to_all | solution.py:505
  87.8 18.9 %shard_map.170 = (bf16[256,2048]{1,0:T(8,128)(2,1)S(1)}, bf16[256,2048]{1,0:T(8,128)(2,1)}) custom-call(bf16[256,2048]{1,0:T(8,128)(2,1)S(1)} %bitcast.21, bf16[256,2048]{1,0:T(8,128)(2,1)} %collective-permute-done.14.oth_ref, bf16[1,2048,1792]{2,1,0:T(8,128)(2,1)} %gate_ref.3, bf16[1,2048,1792]{2,1,0:T(8,128)(2,1)} %up_ref.3, bf16[1,1792,2048]{2,1,0:T(8,128)(2,1)} %down_ref.3), custom_call_target="tpu_custom_call" | custom-call | flops 11274289152 | bytes 22020096 | tf_op jit(solution)/shard_map/pallas_call | solution.py:341
  107.2 2.5 %collective-permute-done.15 = bf16[256,2048]{1,0:T(8,128)(2,1)} collective-permute-done((bf16[256,2048]{1,0:T(8,128)(2,1)}, bf16[256,2048]{1,0:T(8,128)(2,1)}, u32[]{:S(2)}, u32[]{:S(2)}) %collective-permute-start.15) | collective-permute-done | bytes 1048608 | tf_op jit(solution)/shard_map/ppermute | solution.py:513
  109.7 2.6 %add_convert_fusion = bf16[256,2048]{1,0:T(8,128)(2,1)} fusion(bf16[256,2048]{1,0:T(8,128)(2,1)} %collective-permute-done.15, bf16[256,2048]{1,0:T(8,128)(2,1)S(1)} %get-tuple-element.31), kind=kLoop, calls=%fused_computation | loop fusion | flops 2097152 | bytes 3145728 | tf_op jit(solution)/shard_map/convert_element_type | solution.py:514
  112.3 5.0 %all-to-all-start.3 = ((bf16[8,32,2048]{2,1,0:T(8,128)(2,1)}), bf16[8,32,2048]{2,1,0:T(8,128)(2,1)S(1)}, u32[]{:S(2)}, u32[]{:S(2)}) async-start(bf16[8,32,2048]{2,1,0:T(8,128)(2,1)} %bitcast.26), calls=%async_computation.3 | async-start | bytes 2097152 | tf_op jit(solution)/shard_map/all_to_all | solution.py:505
  117.3 17.5 %shard_map.167 = (bf16[256,2048]{1,0:T(8,128)(2,1)S(1)}, bf16[256,2048]{1,0:T(8,128)(2,1)S(1)}) custom-call(bf16[256,2048]{1,0:T(8,128)(2,1)S(1)} %bitcast.19, bf16[256,2048]{1,0:T(8,128)(2,1)S(1)} %collective-permute-done.8.oth_ref, bf16[1,2048,1792]{2,1,0:T(8,128)(2,1)} %gate_ref.3, bf16[1,2048,1792]{2,1,0:T(8,128)(2,1)} %up_ref.3, ...), custom_call_target="tpu_custom_call" | custom-call | flops 11274289152 | bytes 22020096 | tf_op jit(solution)/shard_map/pallas_call | solution.py:341
  134.9 2.6 %collective-permute-done.9 = bf16[256,2048]{1,0:T(8,128)(2,1)S(1)} collective-permute-done((bf16[256,2048]{1,0:T(8,128)(2,1)S(1)}, bf16[256,2048]{1,0:T(8,128)(2,1)S(1)}, u32[]{:S(2)}, u32[]{:S(2)}) %collective-permute-start.9) | collective-permute-done | bytes 1048608 | tf_op jit(solution)/shard_map/ppermute | solution.py:513
  138.9 5.1 %all-to-all-start.1 = ((bf16[8,32,2048]{2,1,0:T(8,128)(2,1)}), bf16[8,32,2048]{2,1,0:T(8,128)(2,1)S(1)}, u32[]{:S(2)}, u32[]{:S(2)}) async-start(bf16[8,32,2048]{2,1,0:T(8,128)(2,1)} %bitcast.7), calls=%async_computation.1 | async-start | bytes 2097152 | tf_op jit(solution)/shard_map/all_to_all | solution.py:505
  147.8 20.5 %all-to-all-done.1 = bf16[8,32,2048]{2,1,0:T(8,128)(2,1)S(1)} async-done(((bf16[8,32,2048]{2,1,0:T(8,128)(2,1)}), bf16[8,32,2048]{2,1,0:T(8,128)(2,1)S(1)}, u32[]{:S(2)}, u32[]{:S(2)}) %all-to-all-start.1) | async-done | bytes 1048608 | tf_op jit(solution)/shard_map/all_to_all | solution.py:505
  169.2 2.6 %collective-permute-done.16.far_ref = bf16[128,2048]{1,0:T(8,128)(2,1)S(1)} collective-permute-done((bf16[128,2048]{1,0:T(8,128)(2,1)}, bf16[128,2048]{1,0:T(8,128)(2,1)S(1)}, u32[]{:S(2)}, u32[]{:S(2)}) %collective-permute-start.16) | collective-permute-done | bytes 524320 | tf_op jit(solution)/shard_map/ppermute | solution.py:536
  (51 shorter events, 14.7 us)
Async XLA Ops:
  0.0 54.7 %collective-permute-start.7 = (bf16[512,2048]{1,0:T(8,128)(2,1)}, bf16[512,2048]{1,0:T(8,128)(2,1)}, u32[]{:S(2)}, u32[]{:S(2)}) collective-permute-start(bf16[512,2048]{1,0:T(8,128)(2,1)} %wa_ref.3), channel_id=1, source_target_pairs={{0,1},{1,0},{2,3},{3,2},{4,5},{5,4},{6,7},{7,6},{8,9},{9,8},{10,11... | collective-permute-start | bytes 6291464 | tf_op jit(solution)/shard_map/ppermute | solution.py:420
  2.8 39.7 %copy-start.6 = (f32[128,2]{0,1:T(2,128)S(1)}, f32[128,2]{0,1:T(2,128)}, u32[]{:S(2)}) copy-start(f32[128,2]{0,1:T(2,128)} %param.27) | copy-start | bytes 3076
  2.8 51.9 %copy-start = (bf16[512,2048]{1,0:T(8,128)(2,1)S(1)}, bf16[512,2048]{1,0:T(8,128)(2,1)}, u32[]{:S(2)}) copy-start(bf16[512,2048]{1,0:T(8,128)(2,1)} %wa_ref.3) | copy-start | bytes 6291460
  2.8 51.9 %copy-start.5 = (f32[2048]{0:T(1024)S(1)}, f32[2048]{0:T(1024)}, u32[]{:S(2)}) copy-start(f32[2048]{0:T(1024)} %param.25) | copy-start | bytes 24580
  2.8 7.2 %collective-permute-start.2 = (bf16[272,128]{1,0:T(8,128)(2,1)S(1)}, bf16[272,128]{1,0:T(8,128)(2,1)S(1)}, u32[]{:S(2)}, u32[]{:S(2)}) collective-permute-start(bf16[272,128]{1,0:T(8,128)(2,1)S(1)} %shard_map.164.own_ref), channel_id=1, source_target_pairs={{0,6},{2,0},{4,2},{6,4},{8,14},{10,8},{12,10},{14,12},{16,22},{18,... | collective-permute-start | bytes 208904 | tf_op jit(solution)/shard_map/ppermute | solution.py:463
  6.3 5.8 %collective-permute-start.1 = (bf16[272,128]{1,0:T(8,128)(2,1)S(1)}, bf16[272,128]{1,0:T(8,128)(2,1)S(1)}, u32[]{:S(2)}, u32[]{:S(2)}) collective-permute-start(bf16[272,128]{1,0:T(8,128)(2,1)S(1)} %shard_map.164.own_ref), channel_id=1, source_target_pairs={{0,4},{2,6},{4,0},{6,2},{8,12},{10,14},{12,8},{14,10},{16,20},{18,... | collective-permute-start | bytes 208904 | tf_op jit(solution)/shard_map/ppermute | solution.py:463
  6.8 5.3 %collective-permute-start = (bf16[272,128]{1,0:T(8,128)(2,1)S(1)}, bf16[272,128]{1,0:T(8,128)(2,1)S(1)}, u32[]{:S(2)}, u32[]{:S(2)}) collective-permute-start(bf16[272,128]{1,0:T(8,128)(2,1)S(1)} %shard_map.164.own_ref), channel_id=1, source_target_pairs={{0,2},{2,4},{4,6},{6,0},{8,10},{10,12},{12,14},{14,8},{16,18},{18,... | collective-permute-start | bytes 208904 | tf_op jit(solution)/shard_map/ppermute | solution.py:463
  7.4 47.3 %collective-permute-start.12 = (bf16[128,2048]{1,0:T(8,128)(2,1)}, bf16[128,2048]{1,0:T(8,128)(2,1)S(1)}, u32[]{:S(2)}, u32[]{:S(2)}) collective-permute-start(bf16[128,2048]{1,0:T(8,128)(2,1)} %res_ref.1), channel_id=1, source_target_pairs={{0,16},{2,18},{4,20},{6,22},{8,24},{10,26},{12,28},{14,30},{16,0},... | collective-permute-start | bytes 1572872 | tf_op jit(solution)/shard_map/ppermute | solution.py:419
  12.3 13.3 %collective-permute-start.5 = (bf16[272,128]{1,0:T(8,128)(2,1)S(1)}, bf16[272,128]{1,0:T(8,128)(2,1)S(1)}, u32[]{:S(2)}, u32[]{:S(2)}) collective-permute-start(bf16[272,128]{1,0:T(8,128)(2,1)S(1)} %get-tuple-element.23), channel_id=1, source_target_pairs={{0,24},{2,26},{4,28},{6,30},{1,25},{3,27},{5,29},{7,31}} | collective-permute-start | bytes 208904 | tf_op jit(solution)/shard_map/ppermute | solution.py:463
  17.8 7.8 %collective-permute-start.4 = (bf16[272,128]{1,0:T(8,128)(2,1)S(1)}, bf16[272,128]{1,0:T(8,128)(2,1)S(1)}, u32[]{:S(2)}, u32[]{:S(2)}) collective-permute-start(bf16[272,128]{1,0:T(8,128)(2,1)S(1)} %get-tuple-element.23), channel_id=1, source_target_pairs={{0,16},{2,18},{4,20},{6,22},{8,24},{10,26},{12,28},{14,30},{1,17},... | collective-permute-start | bytes 208904 | tf_op jit(solution)/shard_map/ppermute | solution.py:463
  19.1 6.6 %collective-permute-start.3 = (bf16[272,128]{1,0:T(8,128)(2,1)S(1)}, bf16[272,128]{1,0:T(8,128)(2,1)S(1)}, u32[]{:S(2)}, u32[]{:S(2)}) collective-permute-start(bf16[272,128]{1,0:T(8,128)(2,1)S(1)} %get-tuple-element.23), channel_id=1, source_target_pairs={{0,8},{2,10},{4,12},{6,14},{8,16},{10,18},{12,20},{14,22},{16,24},... | collective-permute-start | bytes 208904 | tf_op jit(solution)/shard_map/ppermute | solution.py:463
  26.3 28.4 %collective-permute-start.10 = (bf16[128,512]{1,0:T(8,128)(2,1)S(1)}, bf16[128,512]{1,0:T(8,128)(2,1)S(1)}, u32[]{:S(2)}, u32[]{:S(2)}) collective-permute-start(bf16[128,512]{1,0:T(8,128)(2,1)S(1)} %get-tuple-element.24.a_ref), channel_id=1, source_target_pairs={{0,16},{1,17},{2,18},{3,19},{4,20},{5,21},{6,22},{7,23},{8,24},{9,... | collective-permute-start | bytes 393224 | tf_op jit(solution)/shard_map/ppermute | solution.py:490
  42.4 12.3 %collective-permute-start.11 = (bf16[128,512]{1,0:T(8,128)(2,1)S(1)}, bf16[128,512]{1,0:T(8,128)(2,1)S(1)}, u32[]{:S(2)}, u32[]{:S(2)}) collective-permute-start(bf16[128,512]{1,0:T(8,128)(2,1)S(1)} %get-tuple-element.25), channel_id=1, source_target_pairs={{0,17},{1,16},{2,19},{3,18},{4,21},{5,20},{6,23},{7,22},{8,25},{9,... | collective-permute-start | bytes 393224 | tf_op jit(solution)/shard_map/ppermute | solution.py:491
  42.5 12.2 %collective-permute-start.13 = (f32[8,128]{1,0:T(8,128)S(1)}, f32[8,128]{1,0:T(8,128)S(1)}, u32[]{:S(2)}, u32[]{:S(2)}) collective-permute-start(f32[8,128]{1,0:T(8,128)S(1)} %get-tuple-element.33), channel_id=1, source_target_pairs={{0,16},{2,18},{4,20},{6,22},{8,24},{10,26},{12,28},{14,30},{16,0},... | collective-permute-start | bytes 12296 | tf_op jit(solution)/shard_map/ppermute | solution.py:422
  76.5 11.3 %collective-permute-start.14 = (bf16[256,2048]{1,0:T(8,128)(2,1)S(1)}, bf16[256,2048]{1,0:T(8,128)(2,1)}, u32[]{:S(2)}, u32[]{:S(2)}) collective-permute-start(bf16[256,2048]{1,0:T(8,128)(2,1)S(1)} %bitcast.20), channel_id=1, source_target_pairs={{0,1},{1,0},{2,3},{3,2},{4,5},{5,4},{6,7},{7,6},{8,9},{9,8},{10,11... | collective-permute-start | bytes 3145736 | tf_op jit(solution)/shard_map/ppermute | solution.py:511
  76.5 2.8 %collective-permute-start.6 = (bf16[128,512]{1,0:T(8,128)(2,1)S(1)}, bf16[128,512]{1,0:T(8,128)(2,1)S(1)}, u32[]{:S(2)}, u32[]{:S(2)}) collective-permute-start(bf16[128,512]{1,0:T(8,128)(2,1)S(1)} %get-tuple-element.25), channel_id=1, source_target_pairs={{0,1},{1,0},{2,3},{3,2},{4,5},{5,4},{6,7},{7,6},{8,9},{9,8},{10,11... | collective-permute-start | bytes 393224 | tf_op jit(solution)/shard_map/ppermute | solution.py:489
  84.2 22.6 %all-to-all-start = ((bf16[8,32,2048]{2,1,0:T(8,128)(2,1)}), bf16[8,32,2048]{2,1,0:T(8,128)(2,1)S(1)}, u32[]{:S(2)}, u32[]{:S(2)}) async-start(bf16[8,32,2048]{2,1,0:T(8,128)(2,1)} %bitcast.22), calls=%async_computation | async-start | bytes 2097152 | tf_op jit(solution)/shard_map/all_to_all | solution.py:505
  106.7 3.0 %collective-permute-start.15 = (bf16[256,2048]{1,0:T(8,128)(2,1)}, bf16[256,2048]{1,0:T(8,128)(2,1)}, u32[]{:S(2)}, u32[]{:S(2)}) collective-permute-start(bf16[256,2048]{1,0:T(8,128)(2,1)} %get-tuple-element.32), channel_id=1, source_target_pairs={{0,1},{1,0},{2,3},{3,2},{4,5},{5,4},{6,7},{7,6},{8,9},{9,8},{10,11... | collective-permute-start | bytes 3145736 | tf_op jit(solution)/shard_map/ppermute | solution.py:513
  106.8 10.5 %collective-permute-start.8 = (bf16[256,2048]{1,0:T(8,128)(2,1)S(1)}, bf16[256,2048]{1,0:T(8,128)(2,1)S(1)}, u32[]{:S(2)}, u32[]{:S(2)}) collective-permute-start(bf16[256,2048]{1,0:T(8,128)(2,1)S(1)} %bitcast.18), channel_id=1, source_target_pairs={{0,1},{1,0},{2,3},{3,2},{4,5},{5,4},{6,7},{7,6},{8,9},{9,8},{10,11... | collective-permute-start | bytes 3145736 | tf_op jit(solution)/shard_map/ppermute | solution.py:511
  112.3 26.6 %all-to-all-start.3 = ((bf16[8,32,2048]{2,1,0:T(8,128)(2,1)}), bf16[8,32,2048]{2,1,0:T(8,128)(2,1)S(1)}, u32[]{:S(2)}, u32[]{:S(2)}) async-start(bf16[8,32,2048]{2,1,0:T(8,128)(2,1)} %bitcast.26), calls=%async_computation.3 | async-start | bytes 2097152 | tf_op jit(solution)/shard_map/all_to_all | solution.py:505
  134.8 2.7 %collective-permute-start.9 = (bf16[256,2048]{1,0:T(8,128)(2,1)S(1)}, bf16[256,2048]{1,0:T(8,128)(2,1)S(1)}, u32[]{:S(2)}, u32[]{:S(2)}) collective-permute-start(bf16[256,2048]{1,0:T(8,128)(2,1)S(1)} %get-tuple-element.29), channel_id=1, source_target_pairs={{0,1},{1,0},{2,3},{3,2},{4,5},{5,4},{6,7},{7,6},{8,9},{9,8},{10,11... | collective-permute-start | bytes 3145736 | tf_op jit(solution)/shard_map/ppermute | solution.py:513
  138.9 29.4 %all-to-all-start.1 = ((bf16[8,32,2048]{2,1,0:T(8,128)(2,1)}), bf16[8,32,2048]{2,1,0:T(8,128)(2,1)S(1)}, u32[]{:S(2)}, u32[]{:S(2)}) async-start(bf16[8,32,2048]{2,1,0:T(8,128)(2,1)} %bitcast.7), calls=%async_computation.1 | async-start | bytes 2097152 | tf_op jit(solution)/shard_map/all_to_all | solution.py:505
  144.0 27.8 %copy-start.3 = (bf16[128,2048]{1,0:T(8,128)(2,1)S(1)}, bf16[128,2048]{1,0:T(8,128)(2,1)}, u32[]{:S(2)}) copy-start(bf16[128,2048]{1,0:T(8,128)(2,1)} %copy-done.2) | copy-start | bytes 1572868
  145.7 26.1 %collective-permute-start.16 = (bf16[128,2048]{1,0:T(8,128)(2,1)}, bf16[128,2048]{1,0:T(8,128)(2,1)S(1)}, u32[]{:S(2)}, u32[]{:S(2)}) collective-permute-start(bf16[128,2048]{1,0:T(8,128)(2,1)} %shard_map.171), channel_id=1, source_target_pairs={{0,16},{2,18},{4,20},{6,22},{8,24},{10,26},{12,28},{14,30},{16,0},... | collective-permute-start | bytes 1572872 | tf_op jit(solution)/shard_map/ppermute | solution.py:536
  (3 other events, 23.2 us)
where the time goes:
time: 174 us; the launch traced here: 173 us
  Pallas kernels  52.3 us (30%)
  starting transfers between devices  52.1 us (30%)
  waiting for transfers between devices  42.8 us (25%)
  blocking collectives  18.6 us (11%)
  other arithmetic  4.71 us (3%)
  local copies, waits for them, and re-layouts  2.02 us (1%)
    pallas_call x2, Pallas kernels, experts_call(): pl.pallas_call(functools.partial(expert_kernel, first=first), grid=(first...  36.4 us
    all_to_all x3, waiting for transfers between devices, exchange(): lax.all_to_all(x, 'sp', split_axis=0, concat_axis=0, tiled=True, axis_ind...  20.5 us
    all_to_all x1, blocking collectives, exchange(): lax.all_to_all(x, 'sp', split_axis=0, concat_axis=0, tiled=True, axis_ind...  18.6 us
    ppermute x1, starting transfers between devices, shards(): far_a = lax.ppermute(mine, axes, same)  16.1 us
    ppermute x6, starting transfers between devices, shards(): lax.ppermute(own, 'sp', p)  13.9 us
    all_to_all x3, starting transfers between devices, exchange(): lax.all_to_all(x, 'sp', split_axis=0, concat_axis=0, tiled=True, axis_ind...  13.7 us
    pallas_call x6, Pallas kernels, call(): pl.pallas_call(functools.partial(kernel, **static) if static else kernel,...  10.1 us
    ppermute x1, waiting for transfers between devices, shards(): far_meta = lax.ppermute(meta_for((place + half) % count), 'sp', across)  9.93 us
  transfers between devices with their start and end apart: 20, of which 8 were waited for; matrix products, arithmetic and copies ran while one was open for 3% of the time, Pallas kernels for 28%

commit v1 on v0

--- a/solution.py
+++ b/solution.py
@@ -333,7 +333,7 @@
     rows, width = own.shape
     hidden = gate.shape[2]
     tile = next(t for t in (256, 128, hidden) if hidden % t == 0)
-    wide = next(t for t in (512, 256, 128, width) if width % t == 0)
+    wide = next(t for t in (1024, 512, 256, 128, width) if width % t == 0)
     first, last = hidden // tile, width // wide
     whole = pl.BlockSpec((rows, width), lambda i: (0, 0))
     part = pl.BlockSpec((rows, wide), lambda i: (0, jnp.maximum(i - first, 0)))
@@ -351,7 +351,7 @@
         out_specs=[part, part],
         out_shape=[jax.ShapeDtypeStruct((rows, width), BF16)] * 2,
         scratch_shapes=[pltpu.VMEM((2 * rows, hidden), BF16)],
-        compiler_params=params(32),
+        compiler_params=params(24),
         cost_estimate=pl.CostEstimate(
             flops=2 * rows * 6 * width * hidden,
             bytes_accessed=6 * width * hidden,
@@ -372,6 +372,10 @@
 def back_kernel(ret_ref, meta_ref, out_ref, *, capacity, top):
     ids, weights = meta_of(meta_ref, top)
     out_ref[...] = gather_sum(ret_ref[...], ids, weights, capacity).astype(out_ref.dtype)
+
+
+def join_kernel(own_ref, back_ref, out_ref):
+    out_ref[...] = (own_ref[...].astype(F32) + back_ref[...].astype(F32)).astype(BF16)
 
 
 def final_kernel(mixed_ref, part_ref, far_ref, out_ref):
@@ -511,7 +515,7 @@
         oth = lax.ppermute(rows, "tp", swap)
         p_own, p_oth = experts_call(rows, oth, gate_experts, up_experts, down_experts)
         back = lax.ppermute(p_oth, "tp", swap)
-        total = (p_own.astype(F32) + back.astype(F32)).astype(BF16)
+        (total,) = call(join_kernel, [(rows.shape, BF16)], (p_own, back), 12)
         return total.reshape(half, capacity, width)
 
     def back(returned, who, dtype):

time: 174 us -> 174 us (level)
  the two profiles are of different devices: /device:TPU:0 before, /device:TPU:12 now
where the time goes in v1:
time: 174 us; the launch traced here: 171 us
  Pallas kernels  56.3 us (32%)
  waiting for transfers between devices  53.8 us (31%)
  starting transfers between devices  36.1 us (21%)
  blocking collectives  19.7 us (11%)
  local copies, waits for them, and re-layouts  3.32 us (2%)
    pallas_call x2, Pallas kernels, experts_call(): pl.pallas_call(functools.partial(expert_kernel, first=first), grid=(first...  36.2 us
    all_to_all x1, blocking collectives, exchange(): lax.all_to_all(x, 'sp', split_axis=0, concat_axis=0, tiled=True, axis_ind...  19.7 us
    all_to_all x3, waiting for transfers between devices, exchange(): lax.all_to_all(x, 'sp', split_axis=0, concat_axis=0, tiled=True, axis_ind...  17.7 us
    ppermute x6, waiting for transfers between devices, shards(): lax.ppermute(own, 'sp', p)  16.2 us
    all_to_all x3, starting transfers between devices, exchange(): lax.all_to_all(x, 'sp', split_axis=0, concat_axis=0, tiled=True, axis_ind...  15.6 us
    pallas_call x8, Pallas kernels, call(): pl.pallas_call(functools.partial(kernel, **static) if static else kernel,...  14.1 us
    ppermute x6, starting transfers between devices, shards(): lax.ppermute(own, 'sp', p)  10.7 us
    ppermute x1, waiting for transfers between devices, shards(): far_meta = lax.ppermute(meta_for((place + half) % count), 'sp', across)  8.52 us
  transfers between devices with their start and end apart: 20, of which 10 were waited for; matrix products, arithmetic and copies ran while one was open for 1% of the time, Pallas kernels for 31%

profile of v1, /device:TPU:12, one launch (start us, length us, event | category | flops | bytes accessed | tf_op | source)
XLA Modules:
  0.0 170.8 jit_solution(7590436081098749963)
XLA Ops:
  0.0 2.4 %shard_map.164.own_ref = bf16[272,128]{1,0:T(8,128)(2,1)S(1)} custom-call(bf16[256,512]{1,0:T(8,128)(2,1)} %refs_0_.3, bf16[256,512]{1,0:T(8,128)(2,1)} %refs_1_.3, f32[8,256]{1,0:T(8,128)} %bitcast.23, f32[16,8,128]{2,1,0:T(8,128)} %constant.53.clone.refs_4_.refs_3_, f32[256,128]{1,0:T(8,128)} %constant.51.clone.refs_5_.refs_4_, ...), custom_call_target="tpu_custom_call" | custom-call | tf_op jit(solution)/shard_map/pallas_call | solution.py:50
  5.4 2.6 %collective-permute-start.12 = (bf16[128,2048]{1,0:T(8,128)(2,1)}, bf16[128,2048]{1,0:T(8,128)(2,1)S(1)}, u32[]{:S(2)}, u32[]{:S(2)}) collective-permute-start(bf16[128,2048]{1,0:T(8,128)(2,1)} %res_ref.1), channel_id=1, source_target_pairs={{0,16},{2,18},{4,20},{6,22},{8,24},{10,26},{12,28},{14,30},{16,0},... | collective-permute-start | bytes 1572872 | tf_op jit(solution)/shard_map/ppermute | solution.py:423
  8.2 2.4 %collective-permute-done.refs_0_ = bf16[272,128]{1,0:T(8,128)(2,1)S(1)} collective-permute-done((bf16[272,128]{1,0:T(8,128)(2,1)S(1)}, bf16[272,128]{1,0:T(8,128)(2,1)S(1)}, u32[]{:S(2)}, u32[]{:S(2)}) %collective-permute-start) | collective-permute-done | bytes 69664 | tf_op jit(solution)/shard_map/ppermute | solution.py:467
  12.1 5.1 %collective-permute-start.4 = (bf16[272,128]{1,0:T(8,128)(2,1)}, bf16[272,128]{1,0:T(8,128)(2,1)S(1)}, u32[]{:S(2)}, u32[]{:S(2)}) collective-permute-start(bf16[272,128]{1,0:T(8,128)(2,1)} %get-tuple-element.23), channel_id=1, source_target_pairs={{0,16},{2,18},{4,20},{6,22},{8,24},{10,26},{12,28},{14,30},{1,17},... | collective-permute-start | bytes 208904 | tf_op jit(solution)/shard_map/ppermute | solution.py:467
  17.2 1.9 %collective-permute-start.3 = (bf16[272,128]{1,0:T(8,128)(2,1)}, bf16[272,128]{1,0:T(8,128)(2,1)S(1)}, u32[]{:S(2)}, u32[]{:S(2)}) collective-permute-start(bf16[272,128]{1,0:T(8,128)(2,1)} %get-tuple-element.23), channel_id=1, source_target_pairs={{0,8},{2,10},{4,12},{6,14},{8,16},{10,18},{12,20},{14,22},{16,24},... | collective-permute-start | bytes 208904 | tf_op jit(solution)/shard_map/ppermute | solution.py:467
  20.1 3.1 %shard_map.163 = (f32[256,512]{1,0:T(8,128)S(1)}, bf16[256,512]{1,0:T(8,128)(2,1)S(1)}, f32[256,512]{1,0:T(8,128)S(1)}) custom-call(bf16[256,512]{1,0:T(8,128)(2,1)} %refs_0_.2, bf16[256,512]{1,0:T(8,128)(2,1)} %refs_0_.3, bf16[256,512]{1,0:T(8,128)(2,1)} %refs_1_.3, f32[8,256]{1,0:T(8,128)} %bitcast.24, f32[16,8,128]{2,1,0:T(8,128)} %constant.53.clone.refs_4_.refs_3_, ...), custom_call_target="tpu_custom_call" | custom-call | tf_op jit(solution)/shard_map/pallas_call | solution.py:50
  23.1 12.2 %collective-permute-done.4.refs_1_ = bf16[272,128]{1,0:T(8,128)(2,1)S(1)} collective-permute-done((bf16[272,128]{1,0:T(8,128)(2,1)}, bf16[272,128]{1,0:T(8,128)(2,1)S(1)}, u32[]{:S(2)}, u32[]{:S(2)}) %collective-permute-start.4) | collective-permute-done | bytes 69664 | tf_op jit(solution)/shard_map/ppermute | solution.py:467
  37.3 1.9 %collective-permute-start.10 = (bf16[128,512]{1,0:T(8,128)(2,1)S(1)}, bf16[128,512]{1,0:T(8,128)(2,1)S(1)}, u32[]{:S(2)}, u32[]{:S(2)}) collective-permute-start(bf16[128,512]{1,0:T(8,128)(2,1)S(1)} %get-tuple-element.24.a_ref), channel_id=1, source_target_pairs={{0,16},{1,17},{2,18},{3,19},{4,20},{5,21},{6,22},{7,23},{8,24},{9,... | collective-permute-start | bytes 393224 | tf_op jit(solution)/shard_map/ppermute | solution.py:494
  40.3 1.8 %collective-permute-start.13 = (f32[8,128]{1,0:T(8,128)S(1)}, f32[8,128]{1,0:T(8,128)S(1)}, u32[]{:S(2)}, u32[]{:S(2)}) collective-permute-start(f32[8,128]{1,0:T(8,128)S(1)} %get-tuple-element.33), channel_id=1, source_target_pairs={{0,16},{2,18},{4,20},{6,22},{8,24},{10,26},{12,28},{14,30},{16,0},... | collective-permute-start | bytes 12296 | tf_op jit(solution)/shard_map/ppermute | solution.py:426
  42.1 8.5 %collective-permute-done.13.meta_ref = f32[8,128]{1,0:T(8,128)S(1)} collective-permute-done((f32[8,128]{1,0:T(8,128)S(1)}, f32[8,128]{1,0:T(8,128)S(1)}, u32[]{:S(2)}, u32[]{:S(2)}) %collective-permute-start.13) | collective-permute-done | bytes 4128 | tf_op jit(solution)/shard_map/ppermute | solution.py:426
  53.0 3.2 %shard_map.170 = (bf16[128,2048]{1,0:T(8,128)(2,1)}, bf16[256,2048]{1,0:T(8,128)(2,1)S(1)}) custom-call(bf16[128,512]{1,0:T(8,128)(2,1)S(1)} %collective-permute-done.10.a_ref, bf16[128,512]{1,0:T(8,128)(2,1)S(1)} %collective-permute-done.11.b_ref, bf16[512,2048]{1,0:T(8,128)(2,1)S(1)} %copy-done, bf16[512,2048]{1,0:T(8,128)(2,1)} %collective-permute-done.7.wb_ref, ...), custom_call_target="tpu_custom_call" | custom-call | tf_op jit(solution)/shard_map/pallas_call | solution.py:27
  56.2 19.7 %all_to_all.20 = bf16[8,32,2048]{2,1,0:T(8,128)(2,1)} all-to-all(bf16[8,32,2048]{2,1,0:T(8,128)(2,1)S(1)} %bitcast.20), channel_id=1, replica_groups={{0,2,4,6,8,10,12,14},{16,18,20,22,24,26,28,30},{1,3,5,7,9,11,13,15},{17..., dimensions={0} | all-to-all | bytes 2097152 | tf_op jit(solution)/shard_map/all_to_all | solution.py:509
  76.4 2.5 %collective-permute-done.6.b_ref = bf16[128,512]{1,0:T(8,128)(2,1)S(1)} collective-permute-done((bf16[128,512]{1,0:T(8,128)(2,1)S(1)}, bf16[128,512]{1,0:T(8,128)(2,1)S(1)}, u32[]{:S(2)}, u32[]{:S(2)}) %collective-permute-start.6) | collective-permute-done | bytes 131104 | tf_op jit(solution)/shard_map/ppermute | solution.py:493
  78.9 4.0 %shard_map.166 = (bf16[128,2048]{1,0:T(8,128)(2,1)S(1)}, bf16[256,2048]{1,0:T(8,128)(2,1)}) custom-call(bf16[128,512]{1,0:T(8,128)(2,1)S(1)} %get-tuple-element.24.a_ref, bf16[128,512]{1,0:T(8,128)(2,1)S(1)} %collective-permute-done.6.b_ref, bf16[512,2048]{1,0:T(8,128)(2,1)S(1)} %copy-done.1, bf16[512,2048]{1,0:T(8,128)(2,1)} %collective-permute-done.7.wb_ref, ...), custom_call_target="tpu_custom_call" | custom-call | tf_op jit(solution)/shard_map/pallas_call | solution.py:27
  83.7 5.4 %all-to-all-start = ((bf16[8,32,2048]{2,1,0:T(8,128)(2,1)}), bf16[8,32,2048]{2,1,0:T(8,128)(2,1)S(1)}, u32[]{:S(2)}, u32[]{:S(2)}) async-start(bf16[8,32,2048]{2,1,0:T(8,128)(2,1)} %bitcast.5), calls=%async_computation | async-start | bytes 2097152 | tf_op jit(solution)/shard_map/all_to_all | solution.py:509
  89.1 18.6 %shard_map.171 = (bf16[256,2048]{1,0:T(8,128)(2,1)S(1)}, bf16[256,2048]{1,0:T(8,128)(2,1)}) custom-call(bf16[256,2048]{1,0:T(8,128)(2,1)} %bitcast.10.own_ref, bf16[256,2048]{1,0:T(8,128)(2,1)} %collective-permute-done.14.oth_ref, bf16[1,2048,1792]{2,1,0:T(8,128)(2,1)} %gate_ref.3, bf16[1,2048,1792]{2,1,0:T(8,128)(2,1)} %up_ref.3, ...), custom_call_target="tpu_custom_call" | custom-call | flops 11274289152 | bytes 22020096 | tf_op jit(solution)/shard_map/pallas_call | solution.py:341
  108.3 2.4 %collective-permute-done.15.back_ref = bf16[256,2048]{1,0:T(8,128)(2,1)S(1)} collective-permute-done((bf16[256,2048]{1,0:T(8,128)(2,1)}, bf16[256,2048]{1,0:T(8,128)(2,1)S(1)}, u32[]{:S(2)}, u32[]{:S(2)}) %collective-permute-start.15) | collective-permute-done | bytes 1048608 | tf_op jit(solution)/shard_map/ppermute | solution.py:517
  111.8 5.1 %all-to-all-start.3 = ((bf16[8,32,2048]{2,1,0:T(8,128)(2,1)}), bf16[8,32,2048]{2,1,0:T(8,128)(2,1)S(1)}, u32[]{:S(2)}, u32[]{:S(2)}) async-start(bf16[8,32,2048]{2,1,0:T(8,128)(2,1)} %bitcast.11), calls=%async_computation.3 | async-start | bytes 2097152 | tf_op jit(solution)/shard_map/all_to_all | solution.py:509
  117.0 17.6 %shard_map.167 = (bf16[256,2048]{1,0:T(8,128)(2,1)S(1)}, bf16[256,2048]{1,0:T(8,128)(2,1)S(1)}) custom-call(bf16[256,2048]{1,0:T(8,128)(2,1)S(1)} %bitcast.19, bf16[256,2048]{1,0:T(8,128)(2,1)} %collective-permute-done.8.oth_ref, bf16[1,2048,1792]{2,1,0:T(8,128)(2,1)} %gate_ref.3, bf16[1,2048,1792]{2,1,0:T(8,128)(2,1)} %up_ref.3, bf16[1,1792,2048]{2,1,0:T(8,128)(2,1)} %down_ref.3), custom_call_target="tpu_custom_call" | custom-call | flops 11274289152 | bytes 22020096 | tf_op jit(solution)/shard_map/pallas_call | solution.py:341
  134.6 2.6 %collective-permute-done.9.back_ref = bf16[256,2048]{1,0:T(8,128)(2,1)S(1)} collective-permute-done((bf16[256,2048]{1,0:T(8,128)(2,1)S(1)}, bf16[256,2048]{1,0:T(8,128)(2,1)S(1)}, u32[]{:S(2)}, u32[]{:S(2)}) %collective-permute-start.9) | collective-permute-done | bytes 1048608 | tf_op jit(solution)/shard_map/ppermute | solution.py:517
  138.5 5.1 %all-to-all-start.1 = ((bf16[8,32,2048]{2,1,0:T(8,128)(2,1)}), bf16[8,32,2048]{2,1,0:T(8,128)(2,1)S(1)}, u32[]{:S(2)}, u32[]{:S(2)}) async-start(bf16[8,32,2048]{2,1,0:T(8,128)(2,1)} %bitcast.7), calls=%async_computation.1 | async-start | bytes 2097152 | tf_op jit(solution)/shard_map/all_to_all | solution.py:509
  145.3 2.0 %collective-permute-start.16 = (bf16[128,2048]{1,0:T(8,128)(2,1)}, bf16[128,2048]{1,0:T(8,128)(2,1)S(1)}, u32[]{:S(2)}, u32[]{:S(2)}) collective-permute-start(bf16[128,2048]{1,0:T(8,128)(2,1)} %shard_map.173), channel_id=1, source_target_pairs={{0,16},{2,18},{4,20},{6,22},{8,24},{10,26},{12,28},{14,30},{16,0},... | collective-permute-start | bytes 1572872 | tf_op jit(solution)/shard_map/ppermute | solution.py:540
  147.4 17.7 %all-to-all-done.1 = bf16[8,32,2048]{2,1,0:T(8,128)(2,1)S(1)} async-done(((bf16[8,32,2048]{2,1,0:T(8,128)(2,1)}), bf16[8,32,2048]{2,1,0:T(8,128)(2,1)S(1)}, u32[]{:S(2)}, u32[]{:S(2)}) %all-to-all-start.1) | async-done | bytes 1048608 | tf_op jit(solution)/shard_map/all_to_all | solution.py:509
  166.1 3.8 %collective-permute-done.16.far_ref = bf16[128,2048]{1,0:T(8,128)(2,1)S(1)} collective-permute-done((bf16[128,2048]{1,0:T(8,128)(2,1)}, bf16[128,2048]{1,0:T(8,128)(2,1)S(1)}, u32[]{:S(2)}, u32[]{:S(2)}) %collective-permute-start.16) | collective-permute-done | bytes 524320 | tf_op jit(solution)/shard_map/ppermute | solution.py:540
  (49 shorter events, 18.9 us)
Async XLA Ops:
  0.0 78.9 %copy-start.1 = (bf16[512,2048]{1,0:T(8,128)(2,1)S(1)}, bf16[512,2048]{1,0:T(8,128)(2,1)}, u32[]{:S(2)}) copy-start(bf16[512,2048]{1,0:T(8,128)(2,1)} %wa_ref.3) | copy-start | bytes 6291460
  0.0 78.9 %copy-start.4 = (bf16[128,2048]{1,0:T(8,128)(2,1)S(1)}, bf16[128,2048]{1,0:T(8,128)(2,1)}, u32[]{:S(2)}) copy-start(bf16[128,2048]{1,0:T(8,128)(2,1)} %res_ref.1) | copy-start | bytes 1572868
  0.0 50.7 %collective-permute-start.7 = (bf16[512,2048]{1,0:T(8,128)(2,1)}, bf16[512,2048]{1,0:T(8,128)(2,1)}, u32[]{:S(2)}, u32[]{:S(2)}) collective-permute-start(bf16[512,2048]{1,0:T(8,128)(2,1)} %wa_ref.3), channel_id=1, source_target_pairs={{0,1},{1,0},{2,3},{3,2},{4,5},{5,4},{6,7},{7,6},{8,9},{9,8},{10,11... | collective-permute-start | bytes 6291464 | tf_op jit(solution)/shard_map/ppermute | solution.py:424
  2.4 5.6 %collective-permute-start.2 = (bf16[272,128]{1,0:T(8,128)(2,1)S(1)}, bf16[272,128]{1,0:T(8,128)(2,1)S(1)}, u32[]{:S(2)}, u32[]{:S(2)}) collective-permute-start(bf16[272,128]{1,0:T(8,128)(2,1)S(1)} %shard_map.164.own_ref), channel_id=1, source_target_pairs={{0,6},{2,0},{4,2},{6,4},{8,14},{10,8},{12,10},{14,12},{16,22},{18,... | collective-permute-start | bytes 208904 | tf_op jit(solution)/shard_map/ppermute | solution.py:467
  3.9 4.3 %collective-permute-start.1 = (bf16[272,128]{1,0:T(8,128)(2,1)S(1)}, bf16[272,128]{1,0:T(8,128)(2,1)S(1)}, u32[]{:S(2)}, u32[]{:S(2)}) collective-permute-start(bf16[272,128]{1,0:T(8,128)(2,1)S(1)} %shard_map.164.own_ref), channel_id=1, source_target_pairs={{0,4},{2,6},{4,0},{6,2},{8,12},{10,14},{12,8},{14,10},{16,20},{18,... | collective-permute-start | bytes 208904 | tf_op jit(solution)/shard_map/ppermute | solution.py:467
  5.4 5.2 %collective-permute-start = (bf16[272,128]{1,0:T(8,128)(2,1)S(1)}, bf16[272,128]{1,0:T(8,128)(2,1)S(1)}, u32[]{:S(2)}, u32[]{:S(2)}) collective-permute-start(bf16[272,128]{1,0:T(8,128)(2,1)S(1)} %shard_map.164.own_ref), channel_id=1, source_target_pairs={{0,2},{2,4},{4,6},{6,0},{8,10},{10,12},{12,14},{14,8},{16,18},{18,... | collective-permute-start | bytes 208904 | tf_op jit(solution)/shard_map/ppermute | solution.py:467
  5.4 45.2 %collective-permute-start.12 = (bf16[128,2048]{1,0:T(8,128)(2,1)}, bf16[128,2048]{1,0:T(8,128)(2,1)S(1)}, u32[]{:S(2)}, u32[]{:S(2)}) collective-permute-start(bf16[128,2048]{1,0:T(8,128)(2,1)} %res_ref.1), channel_id=1, source_target_pairs={{0,16},{2,18},{4,20},{6,22},{8,24},{10,26},{12,28},{14,30},{16,0},... | collective-permute-start | bytes 1572872 | tf_op jit(solution)/shard_map/ppermute | solution.py:423
  11.4 11.7 %collective-permute-start.5 = (bf16[272,128]{1,0:T(8,128)(2,1)}, bf16[272,128]{1,0:T(8,128)(2,1)S(1)}, u32[]{:S(2)}, u32[]{:S(2)}) collective-permute-start(bf16[272,128]{1,0:T(8,128)(2,1)} %get-tuple-element.23), channel_id=1, source_target_pairs={{0,24},{2,26},{4,28},{6,30},{1,25},{3,27},{5,29},{7,31}} | collective-permute-start | bytes 208904 | tf_op jit(solution)/shard_map/ppermute | solution.py:467
  12.1 23.2 %collective-permute-start.4 = (bf16[272,128]{1,0:T(8,128)(2,1)}, bf16[272,128]{1,0:T(8,128)(2,1)S(1)}, u32[]{:S(2)}, u32[]{:S(2)}) collective-permute-start(bf16[272,128]{1,0:T(8,128)(2,1)} %get-tuple-element.23), channel_id=1, source_target_pairs={{0,16},{2,18},{4,20},{6,22},{8,24},{10,26},{12,28},{14,30},{1,17},... | collective-permute-start | bytes 208904 | tf_op jit(solution)/shard_map/ppermute | solution.py:467
  17.2 19.5 %collective-permute-start.3 = (bf16[272,128]{1,0:T(8,128)(2,1)}, bf16[272,128]{1,0:T(8,128)(2,1)S(1)}, u32[]{:S(2)}, u32[]{:S(2)}) collective-permute-start(bf16[272,128]{1,0:T(8,128)(2,1)} %get-tuple-element.23), channel_id=1, source_target_pairs={{0,8},{2,10},{4,12},{6,14},{8,16},{10,18},{12,20},{14,22},{16,24},... | collective-permute-start | bytes 208904 | tf_op jit(solution)/shard_map/ppermute | solution.py:467
  37.3 13.4 %collective-permute-start.10 = (bf16[128,512]{1,0:T(8,128)(2,1)S(1)}, bf16[128,512]{1,0:T(8,128)(2,1)S(1)}, u32[]{:S(2)}, u32[]{:S(2)}) collective-permute-start(bf16[128,512]{1,0:T(8,128)(2,1)S(1)} %get-tuple-element.24.a_ref), channel_id=1, source_target_pairs={{0,16},{1,17},{2,18},{3,19},{4,20},{5,21},{6,22},{7,23},{8,24},{9,... | collective-permute-start | bytes 393224 | tf_op jit(solution)/shard_map/ppermute | solution.py:494
  39.2 11.5 %collective-permute-start.11 = (bf16[128,512]{1,0:T(8,128)(2,1)S(1)}, bf16[128,512]{1,0:T(8,128)(2,1)S(1)}, u32[]{:S(2)}, u32[]{:S(2)}) collective-permute-start(bf16[128,512]{1,0:T(8,128)(2,1)S(1)} %get-tuple-element.25), channel_id=1, source_target_pairs={{0,17},{1,16},{2,19},{3,18},{4,21},{5,20},{6,23},{7,22},{8,25},{9,... | collective-permute-start | bytes 393224 | tf_op jit(solution)/shard_map/ppermute | solution.py:495
  40.3 10.3 %collective-permute-start.13 = (f32[8,128]{1,0:T(8,128)S(1)}, f32[8,128]{1,0:T(8,128)S(1)}, u32[]{:S(2)}, u32[]{:S(2)}) collective-permute-start(f32[8,128]{1,0:T(8,128)S(1)} %get-tuple-element.33), channel_id=1, source_target_pairs={{0,16},{2,18},{4,20},{6,22},{8,24},{10,26},{12,28},{14,30},{16,0},... | collective-permute-start | bytes 12296 | tf_op jit(solution)/shard_map/ppermute | solution.py:426
  50.7 1.6 copy-start
  75.8 13.3 %collective-permute-start.14 = (bf16[256,2048]{1,0:T(8,128)(2,1)}, bf16[256,2048]{1,0:T(8,128)(2,1)}, u32[]{:S(2)}, u32[]{:S(2)}) collective-permute-start(bf16[256,2048]{1,0:T(8,128)(2,1)} %bitcast.10.own_ref), channel_id=1, source_target_pairs={{0,1},{1,0},{2,3},{3,2},{4,5},{5,4},{6,7},{7,6},{8,9},{9,8},{10,11... | collective-permute-start | bytes 3145736 | tf_op jit(solution)/shard_map/ppermute | solution.py:515
  75.8 3.1 %collective-permute-start.6 = (bf16[128,512]{1,0:T(8,128)(2,1)S(1)}, bf16[128,512]{1,0:T(8,128)(2,1)S(1)}, u32[]{:S(2)}, u32[]{:S(2)}) collective-permute-start(bf16[128,512]{1,0:T(8,128)(2,1)S(1)} %get-tuple-element.25), channel_id=1, source_target_pairs={{0,1},{1,0},{2,3},{3,2},{4,5},{5,4},{6,7},{7,6},{8,9},{9,8},{10,11... | collective-permute-start | bytes 393224 | tf_op jit(solution)/shard_map/ppermute | solution.py:493
  83.7 24.0 %all-to-all-start = ((bf16[8,32,2048]{2,1,0:T(8,128)(2,1)}), bf16[8,32,2048]{2,1,0:T(8,128)(2,1)S(1)}, u32[]{:S(2)}, u32[]{:S(2)}) async-start(bf16[8,32,2048]{2,1,0:T(8,128)(2,1)} %bitcast.5), calls=%async_computation | async-start | bytes 2097152 | tf_op jit(solution)/shard_map/all_to_all | solution.py:509
  107.7 2.9 %collective-permute-start.15 = (bf16[256,2048]{1,0:T(8,128)(2,1)}, bf16[256,2048]{1,0:T(8,128)(2,1)S(1)}, u32[]{:S(2)}, u32[]{:S(2)}) collective-permute-start(bf16[256,2048]{1,0:T(8,128)(2,1)} %get-tuple-element.32), channel_id=1, source_target_pairs={{0,1},{1,0},{2,3},{3,2},{4,5},{5,4},{6,7},{7,6},{8,9},{9,8},{10,11... | collective-permute-start | bytes 3145736 | tf_op jit(solution)/shard_map/ppermute | solution.py:517
  107.8 9.2 %collective-permute-start.8 = (bf16[256,2048]{1,0:T(8,128)(2,1)S(1)}, bf16[256,2048]{1,0:T(8,128)(2,1)}, u32[]{:S(2)}, u32[]{:S(2)}) collective-permute-start(bf16[256,2048]{1,0:T(8,128)(2,1)S(1)} %bitcast.18), channel_id=1, source_target_pairs={{0,1},{1,0},{2,3},{3,2},{4,5},{5,4},{6,7},{7,6},{8,9},{9,8},{10,11... | collective-permute-start | bytes 3145736 | tf_op jit(solution)/shard_map/ppermute | solution.py:515
  111.8 26.6 %all-to-all-start.3 = ((bf16[8,32,2048]{2,1,0:T(8,128)(2,1)}), bf16[8,32,2048]{2,1,0:T(8,128)(2,1)S(1)}, u32[]{:S(2)}, u32[]{:S(2)}) async-start(bf16[8,32,2048]{2,1,0:T(8,128)(2,1)} %bitcast.11), calls=%async_computation.3 | async-start | bytes 2097152 | tf_op jit(solution)/shard_map/all_to_all | solution.py:509
  134.5 35.4 %copy-start.3 = (bf16[128,2048]{1,0:T(8,128)(2,1)S(1)}, bf16[128,2048]{1,0:T(8,128)(2,1)}, u32[]{:S(2)}) copy-start(bf16[128,2048]{1,0:T(8,128)(2,1)} %copy-done.2) | copy-start | bytes 1572868
  134.5 2.7 %collective-permute-start.9 = (bf16[256,2048]{1,0:T(8,128)(2,1)S(1)}, bf16[256,2048]{1,0:T(8,128)(2,1)S(1)}, u32[]{:S(2)}, u32[]{:S(2)}) collective-permute-start(bf16[256,2048]{1,0:T(8,128)(2,1)S(1)} %get-tuple-element.29), channel_id=1, source_target_pairs={{0,1},{1,0},{2,3},{3,2},{4,5},{5,4},{6,7},{7,6},{8,9},{9,8},{10,11... | collective-permute-start | bytes 3145736 | tf_op jit(solution)/shard_map/ppermute | solution.py:517
  138.5 26.6 %all-to-all-start.1 = ((bf16[8,32,2048]{2,1,0:T(8,128)(2,1)}), bf16[8,32,2048]{2,1,0:T(8,128)(2,1)S(1)}, u32[]{:S(2)}, u32[]{:S(2)}) async-start(bf16[8,32,2048]{2,1,0:T(8,128)(2,1)} %bitcast.7), calls=%async_computation.1 | async-start | bytes 2097152 | tf_op jit(solution)/shard_map/all_to_all | solution.py:509
  145.3 24.6 %collective-permute-start.16 = (bf16[128,2048]{1,0:T(8,128)(2,1)}, bf16[128,2048]{1,0:T(8,128)(2,1)S(1)}, u32[]{:S(2)}, u32[]{:S(2)}) collective-permute-start(bf16[128,2048]{1,0:T(8,128)(2,1)} %shard_map.173), channel_id=1, source_target_pairs={{0,16},{2,18},{4,20},{6,22},{8,24},{10,26},{12,28},{14,30},{16,0},... | collective-permute-start | bytes 1572872 | tf_op jit(solution)/shard_map/ppermute | solution.py:540
  (2 other events, 1.5 us)
